TPU v7x, 32 devices: a whole 2x2x4 slice. The times are simulated.
32 devices in a mesh: rep: 4 (over z), fs: 4 (over y, x), tp: 2 (over core).
Axes of the slice: x: 2, y: 2, z: 4, core: 2. Of those that a mesh axis runs over, the one named last changes fastest.
Arguments:
- tokens_in: bfloat16 [8192, 2048], P(('rep', 'fs', 'tp')), may hold values from -6 to 6
- norm_gain: float32 [2048], replicated, may hold values from 0.1 to 1.9
- gate_weight: bfloat16 [2048, 3072], P(None, ('fs', 'tp')), may hold values from -0.125 to 0.125
- up_weight: bfloat16 [2048, 3072], P(None, ('fs', 'tp')), may hold values from -0.125 to 0.125
- down_weight: bfloat16 [3072, 2048], P(('fs', 'tp')), may hold values from -0.109375 to 0.109375
- out_grad: bfloat16 [8192, 2048], P(('rep', 'fs', 'tp')), may hold values from -6 to 6
Outputs:
- grad_in: bfloat16 [8192, 2048], P(('rep', 'fs', 'tp'))
- grad_gain: float32 [2048], replicated
- grad_gate: float32 [2048, 3072], P(None, ('fs', 'tp'))
- grad_up: float32 [2048, 3072], P(None, ('fs', 'tp'))
- grad_down: float32 [3072, 2048], P(('fs', 'tp'))
All inputs are finite; a program needn't handle non-finite values.
Results may differ from a plain program's by a relative error of at most 0.014.
Values may be sent and summed in bfloat16 or wider, within the bound.
A program may use at most 192 MiB of HBM per device.

v0:
```python
import jax
import jax.numpy as jnp
from jax import lax
from jax.sharding import PartitionSpec as P

norm_eps = 1e-06


def shards(tokens_in, norm_gain, gate_weight, up_weight, down_weight, out_grad):
    row_count = tokens_in.shape[0]
    total_tokens = row_count * lax.axis_size("rep") * lax.axis_size("fs") * lax.axis_size("tp")
    factor = float(total_tokens) ** (-0.5)
    whole_in, whole_grad = (
        lax.all_gather(tokens_in, ("fs", "tp"), axis=0, tiled=True),
        lax.all_gather(out_grad, ("fs", "tp"), axis=0, tiled=True),
    )
    floats = whole_in.astype(jnp.float32)
    inverse = lax.rsqrt(jnp.mean(floats * floats, axis=-1, keepdims=True) + norm_eps)
    unit_rows = floats * inverse
    normed = (unit_rows * norm_gain).astype(jnp.bfloat16)
    gate_pre = jnp.dot(normed, gate_weight, preferred_element_type=jnp.float32)
    up_pre = jnp.dot(normed, up_weight, preferred_element_type=jnp.float32)
    sigma = jax.nn.sigmoid(gate_pre)
    active = gate_pre * sigma
    hidden = (active * up_pre).astype(jnp.bfloat16)
    grad_hidden = 0.5 * jnp.dot(whole_grad, down_weight.T, preferred_element_type=jnp.float32)
    grad_gate_pre = (grad_hidden * up_pre * sigma * (1.0 + gate_pre * (1.0 - sigma))).astype(
        jnp.bfloat16
    )
    grad_up_pre = (grad_hidden * active).astype(jnp.bfloat16)
    result = jnp.dot(grad_gate_pre, gate_weight.T, preferred_element_type=jnp.float32)
    grad_normed = lax.psum_scatter(
        (result + jnp.dot(grad_up_pre, up_weight.T, preferred_element_type=jnp.float32)).astype(
            jnp.bfloat16
        ),
        ("fs", "tp"),
        scatter_dimension=0,
        tiled=True,
    ).astype(jnp.float32)
    local_gate = jnp.dot(normed.T, grad_gate_pre, preferred_element_type=jnp.float32)
    local_up = jnp.dot(normed.T, grad_up_pre, preferred_element_type=jnp.float32)
    local_down = jnp.dot(hidden.T, whole_grad, preferred_element_type=jnp.float32)
    summed_gate = lax.psum(local_gate.astype(jnp.bfloat16), "rep").astype(jnp.float32)
    summed_up = lax.psum(local_up.astype(jnp.bfloat16), "rep").astype(jnp.float32)
    summed_down = lax.psum(local_down.astype(jnp.bfloat16), "rep").astype(jnp.float32)
    grad_gate = summed_gate * factor
    grad_up = summed_up * factor
    grad_down = summed_down * (0.5 * factor)
    position = lax.axis_index("fs") * lax.axis_size("tp") + lax.axis_index("tp")
    own_unit = lax.dynamic_slice_in_dim(unit_rows, position * row_count, row_count, 0)
    own_inverse = lax.dynamic_slice_in_dim(inverse, position * row_count, row_count, 0)
    gain_local = jnp.sum(grad_normed * own_unit, axis=0)
    gain_partial = lax.psum(gain_local, ("fs", "tp"))
    grad_gain = lax.psum(gain_partial, "rep")
    scaled = grad_normed * norm_gain
    grad_in = (
        out_grad.astype(jnp.float32)
        + own_inverse * scaled
        - own_unit * own_inverse * jnp.mean(scaled * own_unit, axis=-1, keepdims=True)
    )
    return (grad_in.astype(jnp.bfloat16), grad_gain, grad_gate, grad_up, grad_down)


def solution(mesh):
    in_specs = (
        P(("rep", "fs", "tp"), None),
        P(),
        P(None, ("fs", "tp")),
        P(None, ("fs", "tp")),
        P(("fs", "tp"), None),
        P(("rep", "fs", "tp"), None),
    )
    out_specs = (
        P(("rep", "fs", "tp"), None),
        P(),
        P(None, ("fs", "tp")),
        P(None, ("fs", "tp")),
        P(("fs", "tp"), None),
    )
    return jax.shard_map(shards, mesh=mesh, in_specs=in_specs, out_specs=out_specs, check_vma=False)
```

profile of v0, /device:TPU:0, one launch (start us, length us, event | category | flops | bytes accessed | tf_op | source)
XLA Modules:
  0.0 437.0 jit_solution(11326514007255932176)
XLA Ops:
  7.2 0.0 copy-start
  7.2 0.0 all-gather.3.cloned.1.call-start
  7.2 0.0 copy-start.3
  7.2 0.7 all-gather.3.cloned.1.call-update
  7.9 0.0 all-gather.5.cloned.1.call-start
  8.0 0.7 all-gather.5.cloned.1.call-update
  8.7 0.0 copy-start.9
  8.7 0.0 all-reduce.3.cloned.1.call-start
  8.7 58.2 %all-gather.3.cloned.1.call-done = bf16[2048,2048]{1,0:T(8,128)(2,1)} async-done(((bf16[256,2048]{1,0:T(8,128)(2,1)}), bf16[2048,2048]{1,0:T(8,128)(2,1)}) %all-gather.3.cloned.1.call-update) | async-done | bytes 8388624 | tf_op jit(solution)/shard_map/all_gather | solution.py:14
  66.9 0.0 copy-start.1
  66.9 5.2 %fusion = f32[2048]{0:T(1024)S(1)} fusion(bf16[2048,2048]{1,0:T(8,128)(2,1)} %all-gather.3.cloned.1.call-done), kind=kLoop, calls=%fused_computation.2 | loop fusion | flops 12580864 | bytes 8396800 | tf_op jit(solution)/shard_map/reduce_sum | solution.py:18
  72.1 0.0 copy-done.3
  72.1 0.0 copy-done.9
  72.2 0.5 copy-done.1
  72.7 6.4 %fusion.12 = f32[2048,384]{1,0:T(8,128)} fusion(bf16[2048,384]{1,0:T(8,128)(2,1)S(1)} %copy-done.3, f32[2048]{0:T(1024)S(1)} %copy-done.9, f32[2048]{0:T(1024)S(1)} %add_rsqrt_fusion, bf16[2048,2048]{1,0:T(8,128)(2,1)S(1)} %copy-done.1), kind=kOutput, calls=%fused_computation.30 | convolution fusion | flops 3238002688 | bytes 13123584 | tf_op jit(solution)/shard_map/dot_general | solution.py:22
  79.0 0.0 copy-done
  79.0 6.3 %fusion.11 = f32[2048,384]{1,0:T(8,128)} fusion(bf16[2048,384]{1,0:T(8,128)(2,1)S(1)} %copy-done, f32[2048]{0:T(1024)S(1)} %copy-done.9, f32[2048]{0:T(1024)S(1)} %add_rsqrt_fusion, bf16[2048,2048]{1,0:T(8,128)(2,1)S(1)} %copy-done.1), kind=kOutput, calls=%fused_computation.29 | convolution fusion | flops 3238002688 | bytes 13123584 | tf_op jit(solution)/shard_map/dot_general | solution.py:21
  85.4 37.7 %all-gather.5.cloned.1.call-done = bf16[2048,2048]{1,0:T(8,128)(2,1)} async-done(((bf16[256,2048]{1,0:T(8,128)(2,1)}), bf16[2048,2048]{1,0:T(8,128)(2,1)}) %all-gather.5.cloned.1.call-update) | async-done | bytes 8388624 | tf_op jit(solution)/shard_map/all_gather | solution.py:15
  123.1 0.0 copy-start.10
  123.1 0.0 copy-start.11
  123.1 0.0 copy-start.12
  123.1 0.0 slice-start
  123.1 10.3 %convolution_convert_fusion = bf16[384,2048]{1,0:T(8,128)(2,1)} fusion(bf16[2048,2048]{1,0:T(8,128)(2,1)} %all-gather.5.cloned.1.call-done, f32[2048,384]{1,0:T(8,128)} %fusion.12, f32[2048,384]{1,0:T(8,128)} %fusion.11), kind=kOutput, calls=%fused_computation.14 | convolution fusion | flops 3226730496 | bytes 16252928 | tf_op jit(solution)/shard_map/dot_general | solution.py:42
  133.4 0.0 copy-done.10
  133.4 0.0 copy-done.11
  133.4 0.0 copy-done.12
  133.4 0.0 slice-start.1
  133.4 7.5 %multiply_convert_fusion.2 = (bf16[2048,384]{1,0:T(8,128)(2,1)S(1)}, bf16[2048,384]{1,0:T(8,128)(2,1)S(1)}) fusion(f32[2048,384]{1,0:T(8,128)} %fusion.11, f32[2048,384]{1,0:T(8,128)S(1)} %copy-done.12, bf16[2048,2048]{1,0:T(8,128)(2,1)S(1)} %copy-done.10, bf16[384,2048]{1,0:T(8,128)(2,1)S(1)} %copy-done.11), kind=kOutput, calls=%fused_computation.9 | convolution fusion | flops 3232235520 | bytes 19398656 | tf_op jit(solution)/shard_map/dot_general | solution.py:26
  140.9 0.0 copy-start.6
  140.9 0.0 copy-start.8
  140.9 0.0 slice-done
  141.0 0.0 slice-done.1
  141.0 6.1 %convolution_convert_fusion.1 = bf16[2048,384]{1,0:T(8,128)(2,1)} fusion(bf16[2048,384]{1,0:T(8,128)(2,1)S(1)} %get-tuple-element.10, f32[2048]{0:T(1024)S(1)} %copy-done.9, f32[2048]{0:T(1024)S(1)} %add_rsqrt_fusion, bf16[2048,2048]{1,0:T(8,128)(2,1)S(1)} %bitcast.12), kind=kOutput, calls=%fused_computation.15 | convolution fusion | flops 3238789120 | bytes 11550720 | tf_op jit(solution)/shard_map/dot_general | solution.py:41
  147.1 0.0 copy-done.6
  147.1 0.0 copy-done.8
  147.1 6.0 %convolution_convert_fusion.2 = bf16[2048,384]{1,0:T(8,128)(2,1)} fusion(bf16[2048,384]{1,0:T(8,128)(2,1)S(1)} %get-tuple-element.11, f32[2048]{0:T(1024)S(1)} %copy-done.9, f32[2048]{0:T(1024)S(1)} %add_rsqrt_fusion, bf16[2048,2048]{1,0:T(8,128)(2,1)S(1)} %bitcast.12), kind=kOutput, calls=%fused_computation.16 | convolution fusion | flops 3238789120 | bytes 11550720 | tf_op jit(solution)/shard_map/dot_general | solution.py:40
  153.1 0.0 all-reduce.3.cloned.1.call-update
  153.1 0.3 reduce-scatter.2.cloned.1.call-start
  153.4 0.0 copy-start.7
  153.4 10.1 %fusion.13 = f32[2048,2048]{1,0:T(8,128)} fusion(bf16[2048,384]{1,0:T(8,128)(2,1)} %copy-done.8, bf16[2048,384]{1,0:T(8,128)(2,1)S(1)} %copy-done), kind=kOutput, calls=%fused_computation.31 | convolution fusion | flops 3221225472 | bytes 19922944 | tf_op jit(solution)/shard_map/dot_general | solution.py:31
  163.5 0.0 copy-done.7
  163.5 10.3 %add_convert_fusion = bf16[2048,2048]{1,0:T(8,128)(2,1)} fusion(f32[2048,2048]{1,0:T(8,128)} %fusion.13, bf16[2048,384]{1,0:T(8,128)(2,1)S(1)} %copy-done.7, bf16[2048,384]{1,0:T(8,128)(2,1)S(1)} %copy-done.3), kind=kOutput, calls=%fused_computation.3 | convolution fusion | flops 3229614080 | bytes 28311552 | tf_op jit(solution)/shard_map/dot_general | solution.py:33
  173.8 0.0 reduce-scatter.2.cloned.1.call-update
  173.9 0.1 dynamic-slice.3
  174.0 10.4 %convert_multiply_fusion = f32[2048,2048]{1,0:T(8,128)} fusion(bf16[2048,2048]{1,0:T(8,128)(2,1)} %all-gather.3.cloned.1.call-done, f32[2048]{0:T(1024)S(1)} %add_rsqrt_fusion), kind=kLoop, calls=%fused_computation | loop fusion | flops 8388608 | bytes 25174016 | tf_op jit(solution)/shard_map/mul | solution.py:19
  184.3 141.0 %all-reduce.3.cloned.1.call-done = (bf16[2048,384]{1,0:T(8,128)(2,1)}, bf16[2048,384]{1,0:T(8,128)(2,1)}, bf16[384,2048]{1,0:T(8,128)(2,1)}) async-done(((bf16[2048,384]{1,0:T(8,128)(2,1)}, bf16[2048,384]{1,0:T(8,128)(2,1)}, bf16[384,2048]{1,0:T(8,128)(2,1)}), (bf16[2048,384]{1,0:T(8,128)(2,1)}, bf16[2048,384]{1,0:T(8,128)(2,1)}, bf16[384,2048]{1,0:T(8,128)(2,1)})) %all-reduce.3.cloned.1.call-update) | async-done | bytes 4718608 | tf_op jit(solution)/shard_map/psum | solution.py:43
  325.3 0.0 copy-start.4
  325.3 0.0 copy-start.5
  325.3 3.6 convert_multiply_fusion.2
  328.9 0.0 copy-done.4
  328.9 0.0 copy-done.5
  328.9 3.3 convert_multiply_fusion.3
  332.2 0.0 copy-start.2
  332.2 66.9 %reduce-scatter.2.cloned.1.call-done = bf16[256,2048]{1,0:T(8,128)(2,1)} async-done(((bf16[2048,2048]{1,0:T(8,128)(2,1)}), bf16[256,2048]{1,0:T(8,128)(2,1)}) %reduce-scatter.2.cloned.1.call-update) | async-done | bytes 1048592 | tf_op jit(solution)/shard_map/reduce_scatter | solution.py:32
  399.1 2.6 fusion.8
  401.7 12.8 %psum.35 = f32[2048]{0:T(1024)S(1)} all-reduce(f32[2048]{0:T(1024)S(1)} %get-tuple-element.5), channel_id=1, replica_groups=mesh['rep'=4,'fs'=4,'tp'=2] {'fs','tp'}, use_global_device_ids=true, to_apply=%region_4.0 | all-reduce | flops 2048 | bytes 16384 | tf_op jit(solution)/shard_map/psum | solution.py:53
  414.4 12.4 %psum.36 = f32[2048]{0:T(1024)} all-reduce(f32[2048]{0:T(1024)S(1)} %psum.35), channel_id=1, replica_groups=mesh['rep'=4,'fs'=4,'tp'=2] {'rep'}, use_global_device_ids=true, to_apply=%region_5.0 | all-reduce | flops 2048 | bytes 16384 | tf_op jit(solution)/shard_map/psum | solution.py:54
  426.9 0.0 copy-done.2
  426.9 3.6 fusion.6
  (3 shorter events, 0.0 us)
Async XLA Ops:
  7.2 71.8 %copy-start = (bf16[2048,384]{1,0:T(8,128)(2,1)S(1)}, bf16[2048,384]{1,0:T(8,128)(2,1)}, u32[]{:S(2)}) copy-start(bf16[2048,384]{1,0:T(8,128)(2,1)} %param.8) | copy-start | bytes 4718596
  7.2 59.7 %all-gather.3.cloned.1.call-start = ((), (), s32[]{:S(2)}) async-start(), calls=%async_computation.1 | async-start | bytes 9437184 | tf_op jit(solution)/shard_map/all_gather | solution.py:14
  7.2 64.9 %copy-start.3 = (bf16[2048,384]{1,0:T(8,128)(2,1)S(1)}, bf16[2048,384]{1,0:T(8,128)(2,1)}, u32[]{:S(2)}) copy-start(bf16[2048,384]{1,0:T(8,128)(2,1)} %param.9) | copy-start | bytes 4718596
  7.9 115.2 %all-gather.5.cloned.1.call-start = ((), (), s32[]{:S(2)}) async-start(), calls=%async_computation.2 | async-start | bytes 9437184 | tf_op jit(solution)/shard_map/all_gather | solution.py:15
  8.7 63.5 %copy-start.9 = (f32[2048]{0:T(1024)S(1)}, f32[2048]{0:T(1024)}, u32[]{:S(2)}) copy-start(f32[2048]{0:T(1024)} %param.7) | copy-start | bytes 24580
  8.7 316.6 %all-reduce.3.cloned.1.call-start = ((), (), s32[]{:S(2)}) async-start(), calls=%async_computation.4 | async-start | bytes 9437184 | tf_op jit(solution)/shard_map/psum | solution.py:43
  66.9 5.8 %copy-start.1 = (bf16[2048,2048]{1,0:T(8,128)(2,1)S(1)}, bf16[2048,2048]{1,0:T(8,128)(2,1)}, u32[]{:S(2)}) copy-start(bf16[2048,2048]{1,0:T(8,128)(2,1)} %all-gather.3.cloned.1.call-done) | copy-start | bytes 25165828
  123.1 10.4 %copy-start.10 = (bf16[2048,2048]{1,0:T(8,128)(2,1)S(1)}, bf16[2048,2048]{1,0:T(8,128)(2,1)}, u32[]{:S(2)}) copy-start(bf16[2048,2048]{1,0:T(8,128)(2,1)} %all-gather.5.cloned.1.call-done) | copy-start | bytes 25165828
  123.1 10.4 %copy-start.11 = (bf16[384,2048]{1,0:T(8,128)(2,1)S(1)}, bf16[384,2048]{1,0:T(8,128)(2,1)}, u32[]{:S(2)}) copy-start(bf16[384,2048]{1,0:T(8,128)(2,1)} %param.10) | copy-start | bytes 4718596
  123.1 10.4 %copy-start.12 = (f32[2048,384]{1,0:T(8,128)S(1)}, f32[2048,384]{1,0:T(8,128)}, u32[]{:S(2)}) copy-start(f32[2048,384]{1,0:T(8,128)} %fusion.12) | copy-start | bytes 9437188
  123.1 17.9 %slice-start = ((s8[8388608]{0:T(1024)(128)(4,1)}), s8[4194304]{0:T(1024)(128)(4,1)S(1)}, s32[]{:S(2)}) async-start(s8[8388608]{0:T(1024)(128)(4,1)} %bitcast.11), calls=%async_computation.5 | async-start | bytes 8388608
  133.4 7.5 %slice-start.1 = ((s8[8388608]{0:T(1024)(128)(4,1)}), s8[4194304]{0:T(1024)(128)(4,1)S(1)}, s32[]{:S(2)}) async-start(s8[8388608]{0:T(1024)(128)(4,1)} %bitcast.11), calls=%async_computation.6 | async-start | bytes 8388608
  140.9 6.1 %copy-start.6 = (bf16[2048,384]{1,0:T(8,128)(2,1)}, bf16[2048,384]{1,0:T(8,128)(2,1)S(1)}, u32[]{:S(2)}) copy-start(bf16[2048,384]{1,0:T(8,128)(2,1)S(1)} %get-tuple-element.10) | copy-start | bytes 4718596
  140.9 6.1 %copy-start.8 = (bf16[2048,384]{1,0:T(8,128)(2,1)}, bf16[2048,384]{1,0:T(8,128)(2,1)S(1)}, u32[]{:S(2)}) copy-start(bf16[2048,384]{1,0:T(8,128)(2,1)S(1)} %get-tuple-element.11) | copy-start | bytes 4718596
  153.1 246.0 %reduce-scatter.2.cloned.1.call-start = ((), (), s32[]{:S(2)}) async-start(), calls=%async_computation.3 | async-start | bytes 9437184 | tf_op jit(solution)/shard_map/reduce_scatter | solution.py:32
  153.4 10.1 %copy-start.7 = (bf16[2048,384]{1,0:T(8,128)(2,1)S(1)}, bf16[2048,384]{1,0:T(8,128)(2,1)}, u32[]{:S(2)}) copy-start(bf16[2048,384]{1,0:T(8,128)(2,1)} %copy-done.6) | copy-start | bytes 4718596
  325.3 3.6 copy-start.4
  325.3 3.6 copy-start.5
  332.2 94.7 %copy-start.2 = (bf16[256,2048]{1,0:T(8,128)(2,1)S(1)}, bf16[256,2048]{1,0:T(8,128)(2,1)}, u32[]{:S(2)}) copy-start(bf16[256,2048]{1,0:T(8,128)(2,1)} %param.11) | copy-start | bytes 3145732
Sparse Core Ops, SparseCore 0:
  9.9 56.9 all-gather.2
  68.8 54.2 all-gather.4
  153.3 171.9 all-reduce.2
  328.6 70.4 reduce-scatter.1
where the time goes:
time: 437 us
  waiting for transfers between devices  305 us (70%)
  matrix products  63.1 us (14%)
  other arithmetic  28.6 us (7%)
  blocking collectives  25.2 us (6%)
  between operations  13.9 us (3%)
    psum x1, waiting for transfers between devices, shards(): lax.psum(local_gate.astype(jnp.bfloat16), 'rep').astype(jnp.float32)  141 us
    reduce_scatter x1, waiting for transfers between devices, shards(): lax.psum_scatter((result + jnp.dot(grad_up_pre, up_weight.T, preferred_el...  66.9 us
    all_gather x1, waiting for transfers between devices, shards(): lax.all_gather(tokens_in, ('fs', 'tp'), axis=0, tiled=True)  58.2 us
    all_gather x1, waiting for transfers between devices, shards(): lax.all_gather(out_grad, ('fs', 'tp'), axis=0, tiled=True)  37.7 us
    psum x1, blocking collectives, shards(): gain_partial = lax.psum(gain_local, ('fs', 'tp'))  12.8 us
    psum x1, blocking collectives, shards(): grad_gain = lax.psum(gain_partial, 'rep')  12.4 us
    mul x1, other arithmetic, shards(): unit_rows = floats * inverse  10.4 us
    dot_general x1, matrix products, shards(): jnp.dot(hidden.T, whole_grad, preferred_element_type=jnp.float32)  10.3 us
  transfers between devices with their start and end apart: 4, of which 4 were waited for; matrix products, arithmetic and copies ran while one was open for 13% of the time, Pallas kernels for 0%

commit v1 on v0

--- a/solution.py
+++ b/solution.py
@@ -40,7 +40,9 @@
     local_gate = jnp.dot(normed.T, grad_gate_pre, preferred_element_type=jnp.float32)
     local_up = jnp.dot(normed.T, grad_up_pre, preferred_element_type=jnp.float32)
     local_down = jnp.dot(hidden.T, whole_grad, preferred_element_type=jnp.float32)
-    summed_gate = lax.psum(local_gate.astype(jnp.bfloat16), "rep").astype(jnp.float32)
+    summed_gate = jnp.sum(lax.all_gather(local_gate.astype(jnp.bfloat16), "rep"), axis=0).astype(
+        jnp.float32
+    )
     summed_up = lax.psum(local_up.astype(jnp.bfloat16), "rep").astype(jnp.float32)
     summed_down = lax.psum(local_down.astype(jnp.bfloat16), "rep").astype(jnp.float32)
     grad_gate = summed_gate * factor

time: 437 us -> 498 us (1.14)
  waiting for transfers between devices: 305 us -> 355 us
  other arithmetic: 28.6 us -> 33.9 us
    all_gather x0 -> x1, waiting for transfers between devices: none -> 111 us  [shards(): lax.all_gather(local_gate.astype(jnp.bfloat16), 'rep')]
    psum x1, waiting for transfers between devices: 141 us -> 80.3 us  [shards(): lax.psum(local_up.astype(jnp.bfloat16), 'rep').astype(jnp.float32)]
  transfers between devices with their start and end apart: 4 -> 5, of which waited for: 4 -> 5; matrix products, arithmetic and copies ran while one was open for 13% -> 14% of each run, Pallas kernels for 0% -> 0%
where the time goes in v1:
time: 498 us
  waiting for transfers between devices  355 us (71%)
  matrix products  67.5 us (14%)
  other arithmetic  33.9 us (7%)
  blocking collectives  25.2 us (5%)
  between operations  13.9 us (3%)
    all_gather x1, waiting for transfers between devices, shards(): lax.all_gather(local_gate.astype(jnp.bfloat16), 'rep')  111 us
    psum x1, waiting for transfers between devices, shards(): lax.psum(local_up.astype(jnp.bfloat16), 'rep').astype(jnp.float32)  80.3 us
    reduce_scatter x1, waiting for transfers between devices, shards(): lax.psum_scatter((result + jnp.dot(grad_up_pre, up_weight.T, preferred_el...  66.3 us
    all_gather x1, waiting for transfers between devices, shards(): lax.all_gather(tokens_in, ('fs', 'tp'), axis=0, tiled=True)  58.2 us
    all_gather x1, waiting for transfers between devices, shards(): lax.all_gather(out_grad, ('fs', 'tp'), axis=0, tiled=True)  37.7 us
    psum x1, blocking collectives, shards(): gain_partial = lax.psum(gain_local, ('fs', 'tp'))  12.8 us
    psum x1, blocking collectives, shards(): grad_gain = lax.psum(gain_partial, 'rep')  12.4 us
    dot_general x1, matrix products, shards(): jnp.dot(grad_up_pre, up_weight.T, preferred_element_type=jnp.float32)  10.4 us
  transfers between devices with their start and end apart: 5, of which 5 were waited for; matrix products, arithmetic and copies ran while one was open for 14% of the time, Pallas kernels for 0%

profile of v1, /device:TPU:0, one launch (start us, length us, event | category | flops | bytes accessed | tf_op | source)
XLA Modules:
  0.0 497.5 jit_solution(1765138514429238805)
XLA Ops:
  7.2 0.0 copy-start
  7.2 0.0 all-gather.5.cloned.1.call-start
  7.2 0.0 copy-start.3
  7.2 0.7 all-gather.5.cloned.1.call-update
  7.9 0.0 all-gather.7.cloned.1.call-start
  8.0 0.7 all-gather.7.cloned.1.call-update
  8.7 0.0 copy-start.7
  8.7 0.0 all-reduce.3.cloned.1.call-start
  8.7 58.2 %all-gather.5.cloned.1.call-done = bf16[2048,2048]{1,0:T(8,128)(2,1)} async-done(((bf16[256,2048]{1,0:T(8,128)(2,1)}), bf16[2048,2048]{1,0:T(8,128)(2,1)}) %all-gather.5.cloned.1.call-update) | async-done | bytes 8388624 | tf_op jit(solution)/shard_map/all_gather | solution.py:14
  66.9 0.0 copy-start.1
  66.9 5.2 %fusion = f32[2048]{0:T(1024)S(1)} fusion(bf16[2048,2048]{1,0:T(8,128)(2,1)} %all-gather.5.cloned.1.call-done), kind=kLoop, calls=%fused_computation.2 | loop fusion | flops 12580864 | bytes 8396800 | tf_op jit(solution)/shard_map/reduce_sum | solution.py:18
  72.1 0.0 copy-done.3
  72.1 0.0 copy-done.7
  72.2 0.5 copy-done.1
  72.7 6.4 %fusion.12 = f32[2048,384]{1,0:T(8,128)} fusion(bf16[2048,384]{1,0:T(8,128)(2,1)S(1)} %copy-done.3, f32[2048]{0:T(1024)S(1)} %copy-done.7, f32[2048]{0:T(1024)S(1)} %add_rsqrt_fusion, bf16[2048,2048]{1,0:T(8,128)(2,1)S(1)} %copy-done.1), kind=kOutput, calls=%fused_computation.30 | convolution fusion | flops 3238002688 | bytes 13123584 | tf_op jit(solution)/shard_map/dot_general | solution.py:22
  79.0 0.0 copy-done
  79.0 6.3 %fusion.11 = f32[2048,384]{1,0:T(8,128)} fusion(bf16[2048,384]{1,0:T(8,128)(2,1)S(1)} %copy-done, f32[2048]{0:T(1024)S(1)} %copy-done.7, f32[2048]{0:T(1024)S(1)} %add_rsqrt_fusion, bf16[2048,2048]{1,0:T(8,128)(2,1)S(1)} %copy-done.1), kind=kOutput, calls=%fused_computation.29 | convolution fusion | flops 3238002688 | bytes 13123584 | tf_op jit(solution)/shard_map/dot_general | solution.py:21
  85.4 37.7 %all-gather.7.cloned.1.call-done = bf16[2048,2048]{1,0:T(8,128)(2,1)} async-done(((bf16[256,2048]{1,0:T(8,128)(2,1)}), bf16[2048,2048]{1,0:T(8,128)(2,1)}) %all-gather.7.cloned.1.call-update) | async-done | bytes 8388624 | tf_op jit(solution)/shard_map/all_gather | solution.py:15
  123.1 0.0 copy-start.8
  123.1 0.0 copy-start.9
  123.1 0.0 copy-start.10
  123.1 0.0 slice-start
  123.1 10.3 %convolution_convert_fusion = bf16[384,2048]{1,0:T(8,128)(2,1)} fusion(bf16[2048,2048]{1,0:T(8,128)(2,1)} %all-gather.7.cloned.1.call-done, f32[2048,384]{1,0:T(8,128)} %fusion.12, f32[2048,384]{1,0:T(8,128)} %fusion.11), kind=kOutput, calls=%fused_computation.14 | convolution fusion | flops 3226730496 | bytes 16252928 | tf_op jit(solution)/shard_map/dot_general | solution.py:42
  133.4 0.0 copy-done.8
  133.4 0.0 copy-done.9
  133.4 0.0 copy-done.10
  133.4 0.0 slice-start.1
  133.4 8.3 %multiply_convert_fusion.2 = (bf16[2048,384]{1,0:T(8,128)(2,1)S(1)}, bf16[2048,384]{1,0:T(8,128)(2,1)}) fusion(f32[2048,384]{1,0:T(8,128)} %fusion.11, f32[2048,384]{1,0:T(8,128)S(1)} %copy-done.10, bf16[2048,2048]{1,0:T(8,128)(2,1)S(1)} %copy-done.8, bf16[384,2048]{1,0:T(8,128)(2,1)S(1)} %copy-done.9), kind=kOutput, calls=%fused_computation.9 | convolution fusion | flops 3232235520 | bytes 19398656 | tf_op jit(solution)/shard_map/dot_general | solution.py:26
  141.8 0.0 copy-start.4
  141.8 1.1 copy-done.4
  142.9 0.0 slice-done
  142.9 0.0 slice-done.1
  142.9 6.1 %convolution_convert_fusion.1 = bf16[2048,384]{1,0:T(8,128)(2,1)} fusion(bf16[2048,384]{1,0:T(8,128)(2,1)S(1)} %get-tuple-element.9, f32[2048]{0:T(1024)S(1)} %copy-done.7, f32[2048]{0:T(1024)S(1)} %add_rsqrt_fusion, bf16[2048,2048]{1,0:T(8,128)(2,1)S(1)} %bitcast.13), kind=kOutput, calls=%fused_computation.15 | convolution fusion | flops 3238789120 | bytes 11550720 | tf_op jit(solution)/shard_map/dot_general | solution.py:41
  149.0 0.0 all-reduce.3.cloned.1.call-update
  149.0 0.0 all-gather.9.cloned.1.call-start
  149.1 9.9 %convolution_convert_fusion.2 = bf16[2048,384]{1,0:T(8,128)(2,1)} fusion(bf16[2048,384]{1,0:T(8,128)(2,1)} %get-tuple-element.10, f32[2048]{0:T(1024)S(1)} %copy-done.7, f32[2048]{0:T(1024)S(1)} %add_rsqrt_fusion, bf16[2048,2048]{1,0:T(8,128)(2,1)} %all-gather.5.cloned.1.call-done), kind=kOutput, calls=%fused_computation.16 | convolution fusion | flops 3238789120 | bytes 11550720 | tf_op jit(solution)/shard_map/dot_general | solution.py:40
  159.0 0.0 all-gather.9.cloned.1.call-update
  159.0 0.3 reduce-scatter.2.cloned.1.call-start
  159.3 0.0 copy-start.5
  159.3 9.8 %fusion.13 = f32[2048,2048]{1,0:T(8,128)} fusion(bf16[2048,384]{1,0:T(8,128)(2,1)} %get-tuple-element.10, bf16[2048,384]{1,0:T(8,128)(2,1)S(1)} %copy-done), kind=kOutput, calls=%fused_computation.31 | convolution fusion | flops 3221225472 | bytes 19922944 | tf_op jit(solution)/shard_map/dot_general | solution.py:31
  169.1 0.0 copy-done.5
  169.1 10.4 %add_convert_fusion = bf16[2048,2048]{1,0:T(8,128)(2,1)} fusion(f32[2048,2048]{1,0:T(8,128)} %fusion.13, bf16[2048,384]{1,0:T(8,128)(2,1)S(1)} %copy-done.5, bf16[2048,384]{1,0:T(8,128)(2,1)S(1)} %copy-done.3), kind=kOutput, calls=%fused_computation.3 | convolution fusion | flops 3229614080 | bytes 28311552 | tf_op jit(solution)/shard_map/dot_general | solution.py:33
  179.5 0.0 reduce-scatter.2.cloned.1.call-update
  179.5 0.1 dynamic-slice.3
  179.6 10.4 %convert_multiply_fusion = f32[2048,2048]{1,0:T(8,128)} fusion(bf16[2048,2048]{1,0:T(8,128)(2,1)} %all-gather.5.cloned.1.call-done, f32[2048]{0:T(1024)S(1)} %add_rsqrt_fusion), kind=kLoop, calls=%fused_computation | loop fusion | flops 8388608 | bytes 25174016 | tf_op jit(solution)/shard_map/mul | solution.py:19
  189.9 80.3 %all-reduce.3.cloned.1.call-done = (bf16[2048,384]{1,0:T(8,128)(2,1)}, bf16[384,2048]{1,0:T(8,128)(2,1)}) async-done(((bf16[2048,384]{1,0:T(8,128)(2,1)}, bf16[384,2048]{1,0:T(8,128)(2,1)}), (bf16[2048,384]{1,0:T(8,128)(2,1)}, bf16[384,2048]{1,0:T(8,128)(2,1)})) %all-reduce.3.cloned.1.call-update) | async-done | bytes 3145744 | tf_op jit(solution)/shard_map/psum | solution.py:46
  270.3 0.0 copy-start.6
  270.3 3.6 convert_multiply_fusion.2
  273.8 0.0 copy-done.6
  273.8 1.9 convert_multiply_fusion.3
  275.8 110.8 %all-gather.9.cloned.1.call-done = bf16[8192,384]{1,0:T(8,128)(2,1)} async-done(((bf16[2048,384]{1,0:T(8,128)(2,1)}), bf16[8192,384]{1,0:T(8,128)(2,1)}) %all-gather.9.cloned.1.call-update) | async-done | bytes 6291472 | tf_op jit(solution)/shard_map/all_gather | solution.py:43
  386.6 4.7 reduce_sum.42
  391.4 1.9 convert_multiply_fusion.4
  393.3 0.0 copy-start.2
  393.3 66.3 %reduce-scatter.2.cloned.1.call-done = bf16[256,2048]{1,0:T(8,128)(2,1)} async-done(((bf16[2048,2048]{1,0:T(8,128)(2,1)}), bf16[256,2048]{1,0:T(8,128)(2,1)}) %reduce-scatter.2.cloned.1.call-update) | async-done | bytes 1048592 | tf_op jit(solution)/shard_map/reduce_scatter | solution.py:32
  459.7 2.6 fusion.8
  462.2 12.8 %psum.28 = f32[2048]{0:T(1024)S(1)} all-reduce(f32[2048]{0:T(1024)S(1)} %get-tuple-element.5), channel_id=1, replica_groups=mesh['rep'=4,'fs'=4,'tp'=2] {'fs','tp'}, use_global_device_ids=true, to_apply=%region_4.0 | all-reduce | flops 2048 | bytes 16384 | tf_op jit(solution)/shard_map/psum | solution.py:55
  475.0 12.4 %psum.29 = f32[2048]{0:T(1024)} all-reduce(f32[2048]{0:T(1024)S(1)} %psum.28), channel_id=1, replica_groups=mesh['rep'=4,'fs'=4,'tp'=2] {'rep'}, use_global_device_ids=true, to_apply=%region_5.0 | all-reduce | flops 2048 | bytes 16384 | tf_op jit(solution)/shard_map/psum | solution.py:56
  487.4 0.0 copy-done.2
  487.4 3.6 fusion.6
  (3 shorter events, 0.0 us)
Async XLA Ops:
  7.2 71.8 %copy-start = (bf16[2048,384]{1,0:T(8,128)(2,1)S(1)}, bf16[2048,384]{1,0:T(8,128)(2,1)}, u32[]{:S(2)}) copy-start(bf16[2048,384]{1,0:T(8,128)(2,1)} %param.8) | copy-start | bytes 4718596
  7.2 59.7 %all-gather.5.cloned.1.call-start = ((), (), s32[]{:S(2)}) async-start(), calls=%async_computation.1 | async-start | bytes 9437184 | tf_op jit(solution)/shard_map/all_gather | solution.py:14
  7.2 64.9 %copy-start.3 = (bf16[2048,384]{1,0:T(8,128)(2,1)S(1)}, bf16[2048,384]{1,0:T(8,128)(2,1)}, u32[]{:S(2)}) copy-start(bf16[2048,384]{1,0:T(8,128)(2,1)} %param.9) | copy-start | bytes 4718596
  7.9 115.2 %all-gather.7.cloned.1.call-start = ((), (), s32[]{:S(2)}) async-start(), calls=%async_computation.2 | async-start | bytes 9437184 | tf_op jit(solution)/shard_map/all_gather | solution.py:15
  8.7 63.5 %copy-start.7 = (f32[2048]{0:T(1024)S(1)}, f32[2048]{0:T(1024)}, u32[]{:S(2)}) copy-start(f32[2048]{0:T(1024)} %param.7) | copy-start | bytes 24580
  8.7 261.6 %all-reduce.3.cloned.1.call-start = ((), (), s32[]{:S(2)}) async-start(), calls=%async_computation.5 | async-start | bytes 6291456 | tf_op jit(solution)/shard_map/psum | solution.py:46
  66.9 5.8 %copy-start.1 = (bf16[2048,2048]{1,0:T(8,128)(2,1)S(1)}, bf16[2048,2048]{1,0:T(8,128)(2,1)}, u32[]{:S(2)}) copy-start(bf16[2048,2048]{1,0:T(8,128)(2,1)} %all-gather.5.cloned.1.call-done) | copy-start | bytes 25165828
  123.1 10.3 %copy-start.8 = (bf16[2048,2048]{1,0:T(8,128)(2,1)S(1)}, bf16[2048,2048]{1,0:T(8,128)(2,1)}, u32[]{:S(2)}) copy-start(bf16[2048,2048]{1,0:T(8,128)(2,1)} %all-gather.7.cloned.1.call-done) | copy-start | bytes 25165828
  123.1 10.3 %copy-start.9 = (bf16[384,2048]{1,0:T(8,128)(2,1)S(1)}, bf16[384,2048]{1,0:T(8,128)(2,1)}, u32[]{:S(2)}) copy-start(bf16[384,2048]{1,0:T(8,128)(2,1)} %param.10) | copy-start | bytes 4718596
  123.1 10.4 %copy-start.10 = (f32[2048,384]{1,0:T(8,128)S(1)}, f32[2048,384]{1,0:T(8,128)}, u32[]{:S(2)}) copy-start(f32[2048,384]{1,0:T(8,128)} %fusion.12) | copy-start | bytes 9437188
  123.1 19.8 %slice-start = ((s8[8388608]{0:T(1024)(128)(4,1)}), s8[4194304]{0:T(1024)(128)(4,1)S(1)}, s32[]{:S(2)}) async-start(s8[8388608]{0:T(1024)(128)(4,1)} %bitcast.12), calls=%async_computation.6 | async-start | bytes 8388608
  133.4 9.5 %slice-start.1 = ((s8[8388608]{0:T(1024)(128)(4,1)}), s8[4194304]{0:T(1024)(128)(4,1)S(1)}, s32[]{:S(2)}) async-start(s8[8388608]{0:T(1024)(128)(4,1)} %bitcast.12), calls=%async_computation.7 | async-start | bytes 8388608
  141.8 1.1 copy-start.4
  149.0 237.6 %all-gather.9.cloned.1.call-start = ((), (), s32[]{:S(2)}) async-start(), calls=%async_computation.4 | async-start | bytes 7864320 | tf_op jit(solution)/shard_map/all_gather | solution.py:43
  159.0 300.6 %reduce-scatter.2.cloned.1.call-start = ((), (), s32[]{:S(2)}) async-start(), calls=%async_computation.3 | async-start | bytes 9437184 | tf_op jit(solution)/shard_map/reduce_scatter | solution.py:32
  159.3 9.8 %copy-start.5 = (bf16[2048,384]{1,0:T(8,128)(2,1)S(1)}, bf16[2048,384]{1,0:T(8,128)(2,1)}, u32[]{:S(2)}) copy-start(bf16[2048,384]{1,0:T(8,128)(2,1)} %copy-done.4) | copy-start | bytes 4718596
  270.3 3.6 copy-start.6
  393.3 94.1 %copy-start.2 = (bf16[256,2048]{1,0:T(8,128)(2,1)S(1)}, bf16[256,2048]{1,0:T(8,128)(2,1)}, u32[]{:S(2)}) copy-start(bf16[256,2048]{1,0:T(8,128)(2,1)} %param.11) | copy-start | bytes 3145732
Sparse Core Ops, SparseCore 0:
  9.9 56.9 all-gather.4
  68.8 54.2 all-gather.6
  149.1 121.0 all-reduce.2
  272.3 114.3 all-gather.8
  389.9 69.6 reduce-scatter.1
